TPU v7x, 32 devices: a whole 2x2x4 slice. The times are simulated.
32 devices in a mesh: grp: 2 (over y), kv: 4 (over z), tp: 4 (over x, core).
Axes of the slice: x: 2, y: 2, z: 4, core: 2. Of those that a mesh axis runs over, the one named last changes fastest.
Arguments:
- tokens: bfloat16 [32, 4096], P('grp', 'kv'), parts along dimension 0, may hold values from -16 to 16
- positions: int32 [32], P(('grp', 'kv')), parts along dimension 0, may hold values from 512 to 8191
- state: float32 [32, 16, 128, 128], P(('grp', 'kv'), 'tp'), parts along dimension 0, may hold values from -3 to 3
- norm_gain: float32 [4096], P('kv'), may hold values from 0.1 to 1.9
- w_query: bfloat16 [4096, 2048], P('kv', 'tp'), may hold values from -0.09375 to 0.09375
- w_key: bfloat16 [4096, 2048], P('kv', 'tp'), may hold values from -0.09375 to 0.09375
- w_value: bfloat16 [4096, 2048], P('kv', 'tp'), may hold values from -0.09375 to 0.09375
- w_gate: bfloat16 [4096, 2048], P('kv', 'tp'), may hold values from -0.09375 to 0.09375
- w_out: bfloat16 [2048, 4096], P('tp', 'kv'), may hold values from -0.125 to 0.125
- mlp_gain: float32 [4096], P('kv'), may hold values from 0.1 to 1.9
- w_up: bfloat16 [4096, 16384], P('kv', 'tp'), may hold values from -0.09375 to 0.09375
- w_down: bfloat16 [16384, 4096], P('tp', 'kv'), may hold values from -0.046875 to 0.046875
Outputs:
- layer_out: bfloat16 [32, 4096], P('grp', 'kv'), parts along dimension 0
- new_state: float32 [32, 16, 128, 128], P(('grp', 'kv'), 'tp'), parts along dimension 0
There are 2 independent parts, one for each index of `grp`. A program takes and returns all parts, laid end to end along the dimension named above; an argument that names none is the same for every part. Nothing has to cross between parts.
All inputs are finite; a program needn't handle non-finite values.
Results may differ from a plain program's by a relative error of at most 0.007.
Values may be sent and summed in bfloat16 or wider, within the bound.
A program may use at most 64 MiB of HBM per device.

v0:
```python
import jax
import jax.numpy as jnp
from jax import lax
from jax.sharding import PartitionSpec as P

D = 4096
HEADS = 16


def turn(values, positions):
    half = values.shape[-1] // 2
    freq = 10000.0 ** (-(jnp.arange(half, dtype=jnp.float32) * 2.0) / values.shape[-1])
    angle = positions.astype(jnp.float32)[:, None, None] * freq[None, None, :]
    cosine = jnp.cos(angle)
    sine = jnp.sin(angle)
    first = values[..., :half]
    second = values[..., half:]
    return jnp.concatenate(
        [first * cosine - second * sine, first * sine + second * cosine], axis=-1
    )


def shards(
    tokens,
    positions,
    state,
    norm_gain,
    w_query,
    w_key,
    w_value,
    w_gate,
    w_out,
    mlp_gain,
    w_up,
    w_down,
):
    local_seqs, head_dev, head_size, _ = state.shape
    inputs = tokens.astype(jnp.float32)
    squares = jnp.sum(inputs * inputs, axis=1)
    normed = (inputs * norm_gain).astype(jnp.bfloat16)
    terms = jnp.stack(
        [
            jnp.dot(normed, weight, preferred_element_type=jnp.float32)
            for weight in (w_query, w_key, w_value, w_gate)
        ],
        axis=1,
    )
    summed, total_sq = (
        lax.psum_scatter(terms, "kv", scatter_dimension=0, tiled=True),
        lax.psum_scatter(squares, "kv", scatter_dimension=0, tiled=True),
    )
    scale1 = lax.rsqrt(total_sq / D + 1e-06)
    summed = (summed * scale1[:, None, None]).reshape(local_seqs, 4, head_dev, head_size)
    query = turn(summed[:, 0], positions)
    key_rows = turn(summed[:, 1], positions) * head_size ** (-0.5)
    value = summed[:, 2]
    gate = summed[:, 3]
    heads = (lax.axis_index("tp") * head_dev + jnp.arange(head_dev)).astype(jnp.float32)
    gamma = 1.0 - 2.0 ** (-5.0 - 5.0 * heads / (HEADS - 1))
    new_state = gamma[None, :, None, None] * state + key_rows[:, :, :, None] * value[:, :, None, :]
    read = jnp.einsum("bhd,bhde->bhe", query, new_state, precision=lax.Precision.HIGHEST)
    read = read * lax.rsqrt(jnp.mean(read * read, axis=-1, keepdims=True) + 1e-06)
    retained = (
        (read * jax.nn.silu(gate)).reshape(local_seqs, head_dev * head_size).astype(jnp.bfloat16)
    )
    head_terms = jnp.dot(
        lax.all_gather(retained, "kv", axis=0, tiled=True),
        w_out,
        preferred_element_type=jnp.float32,
    )
    mixed = (inputs + lax.psum(head_terms, "tp")).astype(jnp.bfloat16)
    middle = mixed.astype(jnp.float32)
    squares2 = jnp.sum(middle * middle, axis=1)
    normed2 = (middle * mlp_gain).astype(jnp.bfloat16)
    upward = jnp.dot(normed2, w_up, preferred_element_type=jnp.float32)
    up_full, total_sq2 = lax.psum((upward, squares2), "kv")
    scale2 = lax.rsqrt(total_sq2 / D + 1e-06)
    hidden = jnp.square(jax.nn.relu(up_full * scale2[:, None])).astype(jnp.bfloat16)
    down_terms = jnp.dot(hidden, w_down, preferred_element_type=jnp.float32)
    layer_out = (middle + lax.psum(down_terms, "tp")).astype(jnp.bfloat16)
    return (layer_out, new_state)


def solution(mesh):
    return jax.shard_map(
        shards,
        mesh=mesh,
        in_specs=(
            P("grp", "kv"),
            P(("grp", "kv")),
            P(("grp", "kv"), "tp", None, None),
            P("kv"),
            P("kv", "tp"),
            P("kv", "tp"),
            P("kv", "tp"),
            P("kv", "tp"),
            P("tp", "kv"),
            P("kv"),
            P("kv", "tp"),
            P("tp", "kv"),
        ),
        out_specs=(P("grp", "kv"), P(("grp", "kv"), "tp", None, None)),
        check_vma=False,
    )
```

profile of v0, /device:TPU:0, one launch (start us, length us, event | category | flops | bytes accessed | tf_op | source)
XLA Modules:
  0.0 187.9 jit_solution(12907306079230193447)
XLA Ops:
  7.2 0.0 copy-start
  7.2 0.0 copy-start.2
  7.2 0.0 copy-start.3
  7.2 0.0 all-reduce.13.cloned.1.call-start
  7.2 1.6 convolution_bitcast_fusion.3
  8.8 1.5 convolution_bitcast_fusion.2
  10.3 1.5 convolution_bitcast_fusion.1
  11.8 1.5 convolution_bitcast_fusion
  13.4 0.7 pad_maximum_fusion
  14.0 0.0 all-reduce.13.cloned.1.call-update
  14.1 0.0 all-reduce.7.cloned.1.call-start
  14.1 0.9 fusion.4
  15.0 0.7 convert_element_type.40
  15.7 0.1 multiply_cosine_fusion
  15.8 1.2 dynamic-slice
  17.7 13.5 %all-reduce.1 = f32[16]{0:T(128)S(1)} all-reduce(f32[16]{0:T(128)S(1)} %fusion.4), channel_id=3, replica_groups=mesh['grp'=2,'kv'=4,'tp'=4] {'kv'}, use_global_device_ids=true, to_apply=%region_2.0.clone | all-reduce | flops 16 | bytes 128
  31.2 0.1 fusion.19
  31.3 20.3 %all-reduce.13.cloned.1.call-done = f32[16,4,512]{2,0,1:T(8,128)} async-done(((f32[16,4,512]{2,0,1:T(8,128)}), f32[16,4,512]{2,0,1:T(8,128)}) %all-reduce.13.cloned.1.call-update) | async-done | bytes 131088
  51.6 0.9 dynamic-slice_multiply_fusion
  52.5 0.1 multiply_subtract_fusion
  52.6 0.1 pad_maximum_fusion.1
  52.7 1.6 multiply_add_fusion
  54.3 0.0 copy-start.1
  54.3 1.0 fusion.22
  55.3 0.1 multiply_reduce_fusion
  55.4 0.1 fusion.17
  55.5 13.2 %all-gather = bf16[4,4,512]{2,1,0:T(4,128)(2,1)S(1)} all-gather(bf16[1,4,512]{2,1,0:T(4,128)(2,1)S(1)} %reshape.108), channel_id=1, replica_groups=mesh['grp'=2,'kv'=4,'tp'=4] {'kv'}, dimensions={0}, use_global_device_ids=true | all-gather | bytes 20480 | tf_op jit(solution)/shard_map/all_gather | solution.py:67
  68.7 0.0 copy-done
  68.7 0.9 fusion.23
  69.6 0.0 all-reduce.7.cloned.1.call-update
  69.6 0.0 all-reduce.9.cloned.1.call-start
  69.6 31.3 %all-reduce.7.cloned.1.call-done = f32[16,1024]{1,0:T(8,128)} async-done(((f32[16,1024]{1,0:T(8,128)}), f32[16,1024]{1,0:T(8,128)}) %all-reduce.7.cloned.1.call-update) | async-done | bytes 65552 | tf_op jit(solution)/shard_map/psum | solution.py:71
  101.0 0.0 copy-done.2
  101.0 1.0 fusion.7
  101.9 0.0 copy-done.3
  101.9 5.3 %fusion.9 = f32[16,4096]{1,0:T(8,128)} fusion(bf16[1024,4096]{1,0:T(8,128)(2,1)} %param.22, bf16[16,1024]{1,0:T(8,128)(2,1)S(1)} %get-tuple-element.3, f32[1024]{0:T(1024)S(1)} %copy-done.3), kind=kOutput, calls=%fused_computation.22 | convolution fusion | flops 134266880 | bytes 8687616 | tf_op jit(solution)/shard_map/dot_general | solution.py:75
  107.2 0.0 copy-done.1
  107.2 0.0 all-reduce.9.cloned.1.call-update
  107.2 0.0 all-reduce.11.cloned.1.call-start
  107.3 11.8 %psum.30 = f32[16]{0:T(128)S(1)} all-reduce(f32[16]{0:T(128)S(1)} %get-tuple-element.2), channel_id=1, replica_groups=mesh['grp'=2,'kv'=4,'tp'=4] {'kv'}, use_global_device_ids=true, to_apply=%region_7.8 | all-reduce | flops 16 | bytes 128 | tf_op jit(solution)/shard_map/psum | solution.py:76
  119.1 23.9 %all-reduce.9.cloned.1.call-done = f32[16,4096]{1,0:T(8,128)} async-done(((f32[16,4096]{1,0:T(8,128)}), f32[16,4096]{1,0:T(8,128)}) %all-reduce.9.cloned.1.call-update) | async-done | bytes 262160 | tf_op jit(solution)/shard_map/psum | solution.py:76
  143.0 5.3 %fusion = f32[16,1024]{1,0:T(8,128)} fusion(bf16[4096,1024]{1,0:T(8,128)(2,1)} %param.23, f32[16,4096]{1,0:T(8,128)} %all-reduce.9.cloned.1.call-done, f32[16]{0:T(128)S(1)} %add_rsqrt_fusion.1), kind=kOutput, calls=%fused_computation.6 | convolution fusion | flops 134479872 | bytes 8716352 | tf_op jit(solution)/shard_map/dot_general | solution.py:79
  148.3 0.0 all-reduce.11.cloned.1.call-update
  148.4 31.6 %all-reduce.11.cloned.1.call-done = f32[16,1024]{1,0:T(8,128)} async-done(((f32[16,1024]{1,0:T(8,128)}), f32[16,1024]{1,0:T(8,128)}) %all-reduce.11.cloned.1.call-update) | async-done | bytes 65552 | tf_op jit(solution)/shard_map/psum | solution.py:80
  179.9 1.5 fusion.8
  (8 shorter events, 0.1 us)
Async XLA Ops:
  7.2 61.5 %copy-start = (bf16[512,1024]{1,0:T(8,128)(2,1)S(1)}, bf16[512,1024]{1,0:T(8,128)(2,1)}, u32[]{:S(2)}) copy-start(bf16[512,1024]{1,0:T(8,128)(2,1)} %param.20) | copy-start | bytes 3145732
  7.2 93.8 %copy-start.2 = (bf16[16,1024]{1,0:T(8,128)(2,1)S(1)}, bf16[16,1024]{1,0:T(8,128)(2,1)}, u32[]{:S(2)}) copy-start(bf16[16,1024]{1,0:T(8,128)(2,1)} %param.12) | copy-start | bytes 98308
  7.2 94.7 %copy-start.3 = (f32[1024]{0:T(1024)S(1)}, f32[1024]{0:T(1024)}, u32[]{:S(2)}) copy-start(f32[1024]{0:T(1024)} %param.21) | copy-start | bytes 12292
  7.2 44.4 %all-reduce.13.cloned.1.call-start = ((), (), s32[]{:S(2)}) async-start(), calls=%async_computation.3 | async-start | bytes 262144
  14.1 86.9 %all-reduce.7.cloned.1.call-start = ((), (), s32[]{:S(2)}) async-start(), calls=%async_computation | async-start | bytes 131072 | tf_op jit(solution)/shard_map/psum | solution.py:71
  54.3 52.9 %copy-start.1 = (f32[4,4,128,128]{3,2,1,0:T(8,128)}, f32[4,4,128,128]{3,2,1,0:T(8,128)S(1)}, u32[]{:S(2)}) copy-start(f32[4,4,128,128]{3,2,1,0:T(8,128)S(1)} %multiply_add_fusion) | copy-start | bytes 3145732
  69.6 73.4 %all-reduce.9.cloned.1.call-start = ((), (), s32[]{:S(2)}) async-start(), calls=%async_computation.1 | async-start | bytes 524288 | tf_op jit(solution)/shard_map/psum | solution.py:76
  107.2 72.7 %all-reduce.11.cloned.1.call-start = ((), (), s32[]{:S(2)}) async-start(), calls=%async_computation.2 | async-start | bytes 131072 | tf_op jit(solution)/shard_map/psum | solution.py:80
Sparse Core Ops, SparseCore 0:
  14.2 37.3 all-reduce.12
  69.7 31.1 all-reduce.6
  107.4 35.5 all-reduce.8
  148.5 31.3 all-reduce.10
where the time goes:
time: 189 us; the launch traced here: 188 us
  waiting for transfers between devices  107 us (57%)
  blocking collectives  38.5 us (20%)
  matrix products  18.6 us (10%)
  between operations  14.5 us (8%)
  other arithmetic  7.69 us (4%)
    psum x1, waiting for transfers between devices, shards(): layer_out = (middle + lax.psum(down_terms, 'tp')).astype(jnp.bfloat16)  31.6 us
    psum x1, waiting for transfers between devices, shards(): mixed = (inputs + lax.psum(head_terms, 'tp')).astype(jnp.bfloat16)  31.3 us
    psum x1, waiting for transfers between devices, shards(): up_full, total_sq2 = lax.psum((upward, squares2), 'kv')  23.9 us
    unnamed x5, waiting for transfers between devices  20.4 us
    unnamed x1, blocking collectives  13.5 us
    all_gather x1, blocking collectives, shards(): lax.all_gather(retained, 'kv', axis=0, tiled=True)  13.2 us
    psum x1, blocking collectives, shards(): up_full, total_sq2 = lax.psum((upward, squares2), 'kv')  11.8 us
    dot_general x4, matrix products, shards(): jnp.dot(normed, weight, preferred_element_type=jnp.float32)  6.11 us
  transfers between devices with their start and end apart: 4, of which 4 were waited for; matrix products, arithmetic and copies ran while one was open for 2% of the time, Pallas kernels for 0%

commit v1 on v0

--- a/solution.py
+++ b/solution.py
@@ -5,6 +5,11 @@
 
 D = 4096
 HEADS = 16
+
+
+def gather_and_add(value, name):
+    parts = lax.all_gather(value, name)
+    return jnp.sum(parts, axis=0)
 
 
 def turn(values, positions):
@@ -68,7 +73,7 @@
         w_out,
         preferred_element_type=jnp.float32,
     )
-    mixed = (inputs + lax.psum(head_terms, "tp")).astype(jnp.bfloat16)
+    mixed = (inputs + gather_and_add(head_terms, "tp")).astype(jnp.bfloat16)
     middle = mixed.astype(jnp.float32)
     squares2 = jnp.sum(middle * middle, axis=1)
     normed2 = (middle * mlp_gain).astype(jnp.bfloat16)

time: 189 us -> 161 us (0.85)
  waiting for transfers between devices: 107 us -> 76.6 us
  blocking collectives: 38.5 us -> 43 us
    psum x1 -> x0, waiting for transfers between devices: 31.3 us -> none  [shards(): mixed = (inputs + lax.psum(head_terms, 'tp')).astype(jnp.bfloat16)]
    all_gather x0 -> x1, blocking collectives: none -> 5.77 us  [gather_and_add(): parts = lax.all_gather(value, name)]
    unnamed x5 -> x4, waiting for transfers between devices: 20.4 us -> 20.4 us
  transfers between devices with their start and end apart: 4 -> 3, of which waited for: 4 -> 3; matrix products, arithmetic and copies ran while one was open for 2% -> 2% of each run, Pallas kernels for 0% -> 0%
where the time goes in v1:
time: 161 us; the launch traced here: 160 us
  waiting for transfers between devices  76.6 us (48%)
  blocking collectives  43 us (27%)
  matrix products  18 us (11%)
  between operations  14.5 us (9%)
  other arithmetic  6.87 us (4%)
    psum x1, waiting for transfers between devices, shards(): layer_out = (middle + lax.psum(down_terms, 'tp')).astype(jnp.bfloat16)  31.6 us
    psum x1, waiting for transfers between devices, shards(): up_full, total_sq2 = lax.psum((upward, squares2), 'kv')  24.7 us
    unnamed x4, waiting for transfers between devices  20.4 us
    unnamed x1, blocking collectives  13.5 us
    all_gather x1, blocking collectives, shards(): lax.all_gather(retained, 'kv', axis=0, tiled=True)  13.2 us
    psum x1, blocking collectives, shards(): up_full, total_sq2 = lax.psum((upward, squares2), 'kv')  10.5 us
    dot_general x4, matrix products, shards(): jnp.dot(normed, weight, preferred_element_type=jnp.float32)  6.11 us
    all_gather x1, blocking collectives, gather_and_add(): parts = lax.all_gather(value, name)  5.77 us
  transfers between devices with their start and end apart: 3, of which 3 were waited for; matrix products, arithmetic and copies ran while one was open for 2% of the time, Pallas kernels for 0%

profile of v1, /device:TPU:0, one launch (start us, length us, event | category | flops | bytes accessed | tf_op | source)
XLA Modules:
  0.0 160.4 jit_solution(15602884767458923079)
XLA Ops:
  7.2 0.0 copy-start
  7.2 0.0 copy-start.2
  7.2 0.0 copy-start.3
  7.2 0.0 all-reduce.10.cloned.1.call-start
  7.2 1.6 convolution_bitcast_fusion.3
  8.8 1.5 convolution_bitcast_fusion.2
  10.3 1.5 convolution_bitcast_fusion.1
  11.8 1.5 convolution_bitcast_fusion
  13.4 0.7 pad_maximum_fusion
  14.0 0.0 all-reduce.10.cloned.1.call-update
  14.1 0.0 all-reduce.6.cloned.1.call-start
  14.1 0.9 fusion.4
  15.0 0.7 convert_element_type.40
  15.7 0.1 multiply_cosine_fusion
  15.8 1.2 dynamic-slice
  17.7 13.5 %all-reduce.1 = f32[16]{0:T(128)S(1)} all-reduce(f32[16]{0:T(128)S(1)} %fusion.4), channel_id=4, replica_groups=mesh['grp'=2,'kv'=4,'tp'=4] {'kv'}, use_global_device_ids=true, to_apply=%region_2.0.clone | all-reduce | flops 16 | bytes 128
  31.2 0.1 fusion.19
  31.3 20.3 %all-reduce.10.cloned.1.call-done = f32[16,4,512]{2,0,1:T(8,128)} async-done(((f32[16,4,512]{2,0,1:T(8,128)}), f32[16,4,512]{2,0,1:T(8,128)}) %all-reduce.10.cloned.1.call-update) | async-done | bytes 131088
  51.6 0.9 dynamic-slice_multiply_fusion
  52.5 0.1 multiply_subtract_fusion
  52.6 0.1 pad_maximum_fusion.1
  52.7 1.6 multiply_add_fusion
  54.3 0.0 copy-start.1
  54.3 1.0 fusion.22
  55.3 0.1 multiply_reduce_fusion
  55.4 0.1 fusion.17
  55.5 13.2 %all-gather.1 = bf16[4,4,512]{2,1,0:T(4,128)(2,1)S(1)} all-gather(bf16[1,4,512]{2,1,0:T(4,128)(2,1)S(1)} %reshape.109), channel_id=1, replica_groups=mesh['grp'=2,'kv'=4,'tp'=4] {'kv'}, dimensions={0}, use_global_device_ids=true | all-gather | bytes 20480 | tf_op jit(solution)/shard_map/all_gather | solution.py:72
  68.7 0.0 copy-done
  68.7 0.3 fusion.23
  68.9 5.8 %all-gather = f32[64,1024]{1,0:T(8,128)S(1)} all-gather(f32[16,1024]{1,0:T(8,128)S(1)} %fusion.23), channel_id=2, replica_groups=mesh['grp'=2,'kv'=4,'tp'=4] {'tp'}, dimensions={0}, use_global_device_ids=true | all-gather | bytes 327680 | tf_op jit(solution)/shard_map/all_gather | solution.py:11
  74.7 0.0 copy-done.2
  74.7 0.1 fusion.7
  74.9 0.0 copy-done.3
  74.9 5.3 %fusion.9 = f32[16,4096]{1,0:T(8,128)} fusion(bf16[1024,4096]{1,0:T(8,128)(2,1)} %param.22, bf16[16,1024]{1,0:T(8,128)(2,1)S(1)} %get-tuple-element.3, f32[1024]{0:T(1024)S(1)} %copy-done.3), kind=kOutput, calls=%fused_computation.22 | convolution fusion | flops 134266880 | bytes 8687616 | tf_op jit(solution)/shard_map/dot_general | solution.py:80
  80.2 0.0 copy-done.1
  80.2 0.0 all-reduce.6.cloned.1.call-update
  80.2 0.0 all-reduce.8.cloned.1.call-start
  80.2 10.5 %psum.22 = f32[16]{0:T(128)S(1)} all-reduce(f32[16]{0:T(128)S(1)} %get-tuple-element.2), channel_id=1, replica_groups=mesh['grp'=2,'kv'=4,'tp'=4] {'kv'}, use_global_device_ids=true, to_apply=%region_7.8 | all-reduce | flops 16 | bytes 128 | tf_op jit(solution)/shard_map/psum | solution.py:81
  90.8 24.7 %all-reduce.6.cloned.1.call-done = f32[16,4096]{1,0:T(8,128)} async-done(((f32[16,4096]{1,0:T(8,128)}), f32[16,4096]{1,0:T(8,128)}) %all-reduce.6.cloned.1.call-update) | async-done | bytes 262160 | tf_op jit(solution)/shard_map/psum | solution.py:81
  115.5 5.3 %fusion = f32[16,1024]{1,0:T(8,128)} fusion(bf16[4096,1024]{1,0:T(8,128)(2,1)} %param.23, f32[16,4096]{1,0:T(8,128)} %all-reduce.6.cloned.1.call-done, f32[16]{0:T(128)S(1)} %add_rsqrt_fusion.1), kind=kOutput, calls=%fused_computation.6 | convolution fusion | flops 134479872 | bytes 8716352 | tf_op jit(solution)/shard_map/dot_general | solution.py:84
  120.8 0.0 all-reduce.8.cloned.1.call-update
  120.8 31.6 %all-reduce.8.cloned.1.call-done = f32[16,1024]{1,0:T(8,128)} async-done(((f32[16,1024]{1,0:T(8,128)}), f32[16,1024]{1,0:T(8,128)}) %all-reduce.8.cloned.1.call-update) | async-done | bytes 65552 | tf_op jit(solution)/shard_map/psum | solution.py:85
  152.4 1.5 fusion.8
  (9 shorter events, 0.1 us)
Async XLA Ops:
  7.2 61.5 %copy-start = (bf16[512,1024]{1,0:T(8,128)(2,1)S(1)}, bf16[512,1024]{1,0:T(8,128)(2,1)}, u32[]{:S(2)}) copy-start(bf16[512,1024]{1,0:T(8,128)(2,1)} %param.20) | copy-start | bytes 3145732
  7.2 67.6 %copy-start.2 = (bf16[16,1024]{1,0:T(8,128)(2,1)S(1)}, bf16[16,1024]{1,0:T(8,128)(2,1)}, u32[]{:S(2)}) copy-start(bf16[16,1024]{1,0:T(8,128)(2,1)} %param.12) | copy-start | bytes 98308
  7.2 67.7 %copy-start.3 = (f32[1024]{0:T(1024)S(1)}, f32[1024]{0:T(1024)}, u32[]{:S(2)}) copy-start(f32[1024]{0:T(1024)} %param.21) | copy-start | bytes 12292
  7.2 44.4 %all-reduce.10.cloned.1.call-start = ((), (), s32[]{:S(2)}) async-start(), calls=%async_computation.2 | async-start | bytes 262144
  14.1 101.4 %all-reduce.6.cloned.1.call-start = ((), (), s32[]{:S(2)}) async-start(), calls=%async_computation | async-start | bytes 524288 | tf_op jit(solution)/shard_map/psum | solution.py:81
  54.3 25.9 %copy-start.1 = (f32[4,4,128,128]{3,2,1,0:T(8,128)}, f32[4,4,128,128]{3,2,1,0:T(8,128)S(1)}, u32[]{:S(2)}) copy-start(f32[4,4,128,128]{3,2,1,0:T(8,128)S(1)} %multiply_add_fusion) | copy-start | bytes 3145732
  80.2 72.2 %all-reduce.8.cloned.1.call-start = ((), (), s32[]{:S(2)}) async-start(), calls=%async_computation.1 | async-start | bytes 131072 | tf_op jit(solution)/shard_map/psum | solution.py:85
Sparse Core Ops, SparseCore 0:
  14.2 37.3 all-reduce.9
  80.3 35.0 all-reduce.5
  120.9 31.3 all-reduce.7
